TPU v7x, 32 devices: a whole 2x2x4 slice. The times are simulated.
32 devices in a mesh: ep: 4 (over y, x), tp: 8 (over z, core).
Axes of the slice: x: 2, y: 2, z: 4, core: 2. Of those that a mesh axis runs over, the one named last changes fastest.
Arguments:
- queries: bfloat16 [2048, 16, 128], P('ep', 'tp'), may hold values from -125 to 125
- keys: bfloat16 [2048, 16, 128], P('ep', 'tp'), may hold values from -9 to 9
- values: bfloat16 [2048, 16, 128], P('ep', 'tp'), may hold values from -6 to 6
- mixing: float32 [16], P('tp'), may hold values from 0.3 to 0.8
- head_gain: float32 [128], replicated, may hold values from 0.1 to 1.9
- out_weight: bfloat16 [16, 128, 2048], P('tp'), may hold values from -0.125 to 0.125
- tokens_b: bfloat16 [4096, 2048], P(('ep', 'tp')), may hold values from -6 to 6
- norm_gain: float32 [2048], replicated, may hold values from 0.1 to 1.9
- expert_ids: int32 [4096, 2], P(('ep', 'tp')), may hold values from 0 to 3, all different within a row; in each aligned block of 128 rows (0 to 127, 128 to 255, ...) at most 96 rows name the same one
- group_gate: float32 [4096], P(('ep', 'tp')), may hold values from 0.2 to 1
- expert_gate: float32 [4096, 2], P(('ep', 'tp')), may hold values from 0.1 to 0.9
- gate_weight: bfloat16 [4, 2048, 1024], P('ep', None, 'tp'), may hold values from -0.125 to 0.125
- up_weight: bfloat16 [4, 2048, 1024], P('ep', None, 'tp'), may hold values from -0.125 to 0.125
- down_weight: bfloat16 [4, 2048, 1024], P('ep', None, 'tp'), may hold values from -0.1875 to 0.1875
Outputs:
- mixed: bfloat16 [2048, 2048], P(('ep', 'tp'))
- routed: bfloat16 [4096, 2048], P(('ep', 'tp'))
Inputs may be any that keep to these rules, and one draw needn't show every extreme that they name: `expert_ids`: within each aligned block of 128 rows, no expert is named by more than 96 rows, and some block has an expert named by exactly 96 rows.
All inputs are finite; a program needn't handle non-finite values.
Results may differ from a plain program's by a relative error of at most 0.019.
Values may be sent and summed in bfloat16 or wider, within the bound.
A program may use at most 192 MiB of HBM per device.

v0:
```python
import math
import jax
import jax.numpy as jnp
from jax import lax
from jax.sharding import PartitionSpec as P

HEAD = 64


def attend_heads(queries, keys, values, mixing, head_gain):
    shard_rows = queries.shape[0]
    head_count = queries.shape[1]
    value_width = values.shape[2]
    query_start = lax.axis_index("ep") * shard_rows
    score_scale = 1.0 / math.sqrt(HEAD)
    query_pos = query_start + lax.iota(jnp.int32, shard_rows)

    def update(running, key_block, value_block, block_start):
        key_pos = block_start + lax.iota(jnp.int32, shard_rows)
        allowed = key_pos[None, :] <= query_pos[:, None]
        fresh = []
        for map_index in range(2):
            maximum, row_sum, numerator = running[3 * map_index : 3 * map_index + 3]
            offset = map_index * HEAD
            scores = (
                jnp.einsum(
                    "qhd,khd->hqk",
                    queries[:, :, offset : offset + HEAD],
                    key_block[:, :, offset : offset + HEAD],
                    preferred_element_type=jnp.float32,
                )
                * score_scale
            )
            scores = jnp.where(allowed[None], scores, -1e30)
            newmax = jnp.maximum(maximum, jnp.max(scores, axis=2))
            shrink = jnp.exp(maximum - newmax)
            weights = jnp.exp(scores - newmax[:, :, None])
            row_sum = row_sum * shrink + jnp.sum(weights, axis=2)
            numerator = numerator * shrink[:, :, None] + jnp.einsum(
                "hqk,khe->hqe",
                weights.astype(jnp.bfloat16),
                value_block,
                preferred_element_type=jnp.float32,
            )
            fresh += [newmax, row_sum, numerator]
        return tuple(fresh)

    floor_max = jnp.full((head_count, shard_rows), -1e30, jnp.float32)
    zero_sum = jnp.zeros((head_count, shard_rows), jnp.float32)
    zero_acc = jnp.zeros((head_count, shard_rows, value_width), jnp.float32)
    start_state = (floor_max, zero_sum, zero_acc, floor_max, zero_sum, zero_acc)
    running = start_state
    key_piece = lax.all_gather(keys, "ep", axis=0, tiled=True)
    value_piece = lax.all_gather(values, "ep", axis=0, tiled=True)
    blocks = key_piece.shape[0] // shard_rows
    key_blocks = key_piece.reshape(blocks, shard_rows, head_count, key_piece.shape[2])
    value_blocks = value_piece.reshape(blocks, shard_rows, head_count, value_width)

    def visit_block(state, inputs):
        key_block, value_block, block_index = inputs
        block_start = block_index * shard_rows
        state = lax.cond(
            block_start <= query_start + shard_rows - 1,
            lambda state_in: update(state_in, key_block, value_block, block_start),
            lambda state_in: state_in,
            state,
        )
        return (state, None)

    running, unused = lax.scan(
        visit_block, running, (key_blocks, value_blocks, lax.iota(jnp.int32, blocks))
    )
    state = running
    diff = state[2] / state[1][:, :, None] - mixing[:, None, None] * state[5] / state[4][:, :, None]
    normed = diff * lax.rsqrt(jnp.mean(diff * diff, axis=2, keepdims=True) + 1e-05) * head_gain
    return normed.astype(jnp.bfloat16)


def mixer_half(queries, keys, values, mixing, head_gain, out_weight):
    attended = attend_heads(queries, keys, values, mixing, head_gain)
    return lax.psum_scatter(
        jnp.einsum("hqe,hed->qd", attended, out_weight, preferred_element_type=jnp.float32).astype(
            jnp.bfloat16
        ),
        "tp",
        scatter_dimension=0,
        tiled=True,
    )


def expert_half(
    tokens_b, norm_gain, expert_ids, group_gate, expert_gate, gate_weight, up_weight, down_weight
):
    local_rows = tokens_b.shape[0]
    width = tokens_b.shape[1]
    top_count = expert_ids.shape[1]
    ep_count = lax.axis_size("ep")
    local_count = gate_weight.shape[0]
    expert_total = ep_count * local_count
    capacity = 3 * local_rows * top_count // (2 * expert_total)
    tokens_f = tokens_b.astype(jnp.float32)
    normed = (
        tokens_f
        * lax.rsqrt(jnp.mean(tokens_f * tokens_f, axis=1, keepdims=True) + 1e-06)
        * norm_gain
    ).astype(jnp.bfloat16)
    flat_ids = expert_ids.reshape(-1)
    one_hot = (flat_ids[:, None] == lax.iota(jnp.int32, expert_total)[None, :]).astype(jnp.int32)
    slot_rank = jnp.sum((jnp.cumsum(one_hot, axis=0) - one_hot) * one_hot, axis=1)
    slot_index = flat_ids * capacity + slot_rank
    owners = jnp.full((expert_total * capacity,), local_rows, jnp.int32)
    owners = owners.at[slot_index].set(lax.iota(jnp.int32, local_rows * top_count) // top_count)
    padded = jnp.concatenate([normed, jnp.zeros((1, width), jnp.bfloat16)], axis=0)
    outgoing = padded[owners].reshape(ep_count, local_count * capacity, width)
    incoming = lax.all_to_all(outgoing, "ep", split_axis=0, concat_axis=0, tiled=True)
    expert_rows = jnp.transpose(
        incoming.reshape(ep_count, local_count, capacity, width), (1, 0, 2, 3)
    )
    expert_rows = expert_rows.reshape(local_count, ep_count * capacity, width)
    piece_gate = lax.all_gather(gate_weight, "tp", axis=2, tiled=True)
    piece_up = lax.all_gather(up_weight, "tp", axis=2, tiled=True)
    piece_down = lax.all_gather(down_weight, "tp", axis=2, tiled=True)
    gate_part = jnp.einsum(
        "jrd,jdf->jrf", expert_rows, piece_gate, preferred_element_type=jnp.float32
    )
    up_part = jnp.einsum("jrd,jdf->jrf", expert_rows, piece_up, preferred_element_type=jnp.float32)
    hidden = (jax.nn.silu(gate_part) * up_part).astype(jnp.bfloat16)
    expert_out = jnp.einsum(
        "jrf,jdf->jrd", hidden, piece_down, preferred_element_type=jnp.float32
    ).astype(jnp.bfloat16)
    outbound = jnp.transpose(
        expert_out.reshape(local_count, ep_count, capacity, width), (1, 0, 2, 3)
    )
    outbound = outbound.reshape(ep_count, local_count * capacity, width)
    returned = lax.all_to_all(outbound, "ep", split_axis=0, concat_axis=0, tiled=True).reshape(
        expert_total * capacity, width
    )
    picked = returned[slot_index].reshape(local_rows, top_count, width).astype(jnp.float32)
    route_weight = group_gate[:, None] * expert_gate
    return jnp.sum(route_weight[:, :, None] * picked, axis=1).astype(jnp.bfloat16)


def per_device(
    queries,
    keys,
    values,
    mixing,
    head_gain,
    out_weight,
    tokens_b,
    norm_gain,
    expert_ids,
    group_gate,
    expert_gate,
    gate_weight,
    up_weight,
    down_weight,
):
    mixed = mixer_half(queries, keys, values, mixing, head_gain, out_weight)
    routed = expert_half(
        tokens_b,
        norm_gain,
        expert_ids,
        group_gate,
        expert_gate,
        gate_weight,
        up_weight,
        down_weight,
    )
    return (mixed, routed)


def solution(mesh):
    placed = (
        P("ep", "tp", None),
        P("ep", "tp", None),
        P("ep", "tp", None),
        P("tp"),
        P(),
        P("tp", None, None),
        P(("ep", "tp"), None),
        P(),
        P(("ep", "tp"), None),
        P(("ep", "tp")),
        P(("ep", "tp"), None),
        P("ep", None, "tp"),
        P("ep", None, "tp"),
        P("ep", None, "tp"),
    )
    return jax.shard_map(
        per_device,
        mesh=mesh,
        in_specs=placed,
        out_specs=(P(("ep", "tp"), None), P(("ep", "tp"), None)),
        check_vma=False,
    )
```

profile of v0, /device:TPU:0, one launch (start us, length us, event | category | flops | bytes accessed | tf_op | source)
XLA Modules:
  0.0 260.2 jit_solution(6079203360803837472)
XLA Ops:
  7.2 0.0 copy-start
  7.2 0.0 all-gather.6.cloned.1.call-start
  7.3 1.8 copy.24
  9.1 0.0 all-gather.6.cloned.1.call-update
  9.1 0.0 all-gather.8.cloned.1.call-start
  9.1 1.7 copy.25
  10.8 0.0 all-gather.8.cloned.1.call-update
  10.8 0.0 all-gather.10.cloned.1.call-start
  10.9 0.7 all-gather.10.cloned.1.call-update
  11.6 0.0 all-gather.12.cloned.1.call-start
  11.6 0.5 all-gather.12.cloned.1.call-update
  12.2 0.0 all-gather.14.cloned.1.call-start
  12.2 0.5 all-gather.14.cloned.1.call-update
  12.7 0.0 reduce-scatter.2.cloned.1.call-start
  12.8 0.1 copy.31
  12.9 0.1 eq.29
  13.1 0.1 eq.25
  13.2 0.2 copy.27
  13.4 1.2 reduce-window.6
  14.6 0.1 slice.34
  14.7 0.1 copy.33
  14.9 0.1 copy.34
  15.0 0.1 copy.30
  15.1 0.1 mul.169
  15.2 0.1 add_bitcast_fusion
  15.3 1.4 scatter_custom_fusion
  16.7 0.2 fusion.31
  17.0 1.0 fusion.33
  17.9 21.8 %all-gather.6.cloned.1.call-done = bf16[2048,2,128]{2,0,1:T(8,128)(2,1)} async-done(((bf16[512,2,128]{2,0,1:T(8,128)(2,1)}), bf16[2048,2,128]{2,0,1:T(8,128)(2,1)}) %all-gather.6.cloned.1.call-update) | async-done | bytes 1048592 | tf_op jit(solution)/shard_map/all_gather | solution.py:53
  39.7 2.3 copy.26
  42.0 26.1 %all-gather.8.cloned.1.call-done = bf16[2048,2,128]{2,0,1:T(8,128)(2,1)} async-done(((bf16[512,2,128]{2,0,1:T(8,128)(2,1)}), bf16[2048,2,128]{2,0,1:T(8,128)(2,1)}) %all-gather.8.cloned.1.call-update) | async-done | bytes 1048592 | tf_op jit(solution)/shard_map/all_gather | solution.py:54
  68.1 1.3 copy.28
  69.5 0.0 copy-start.8
  69.5 0.0 copy-start.9
  69.5 9.8 %while.23 = (s32[]{:T(128)}, f32[2,512]{1,0:T(2,128)S(1)}, f32[2,512]{1,0:T(2,128)S(1)}, f32[2,512,128]{2,1,0:T(8,128)S(1)}, f32[2,512]{1,0:T(2,128)S(1)}, /*ind...) while((s32[]{:T(128)}, f32[2,512]{1,0:T(2,128)S(1)}, ...), condition=%wide.region_7.8_spmd.clone, body=%wide.region_0.7_spmd.clone.sunk | while | flops 410784768 | bytes 17183128 | solution.py:70
  69.6 0.6 dynamic_slice.36
  70.8 4.6 %conditional.3 = ((f32[2,512]{1,0:T(2,128)S(1)}, f32[2,512]{1,0:T(2,128)S(1)}, f32[2,512,128]{2,1,0:T(8,128)S(1)}, f32[2,512]{1,0:T(2,128)S(1)}, f32[2,512]{1,0:T(2,128)S(1)}, /*index=5*/f32[2,512,128]{2,1,0:T(8,128)S(1)})) conditional(s32[]{:T(128)} %convert_element_type.87, (f32[2,512]{1,0:T(2,128)S(1)}, f32[2,512]{1,0:T(2,128)S(1)}, ...), branch_computations={%region_1.1_spmd, %region_2.6_spmd} | conditional | flops 410784768 | bytes 17180748 | solution.py:62
  70.8 1.0 dynamic-slice_bitcast_fusion
  71.8 0.2 broadcast_compare_fusion
  72.1 0.6 fusion.45
  72.7 0.3 fusion.3
  73.0 0.6 fusion.46
  73.6 0.3 fusion.5
  74.0 0.7 convolution_add_fusion
  74.7 0.7 convolution_add_fusion.1
  75.5 0.6 dynamic_slice.36
  76.8 0.6 dynamic_slice.36
  78.1 0.6 dynamic_slice.36
  79.4 0.5 multiply_reduce_fusion.1
  79.9 0.0 copy-start.2
  79.9 2.1 bitcast_convert_fusion
  82.0 0.0 reduce-scatter.2.cloned.1.call-update
  82.2 2.5 gather_fusion
  84.6 36.1 %all_to_all.10 = bf16[4,96,2048]{2,1,0:T(8,128)(2,1)} all-to-all(bf16[4,96,2048]{2,1,0:T(8,128)(2,1)S(1)} %bitcast.62), channel_id=1, replica_groups=mesh['ep'=4,'tp'=8] {'ep'}, dimensions={0} | all-to-all | bytes 3145728 | tf_op jit(solution)/shard_map/all_to_all | solution.py:115
  120.7 5.7 %fusion.24 = f32[384,1024]{1,0:T(8,128)} fusion(bf16[384,2048]{1,0:T(8,128)(2,1)} %bitcast.63, bf16[1,2048,1024]{2,1,0:T(8,128)(2,1)} %all-gather.10.cloned.1.call-done), kind=kOutput, calls=%fused_computation.38 | convolution fusion | flops 1610612736 | bytes 7340032 | tf_op jit(solution)/shard_map/jrd,jdf->jrf/dot_general | solution.py:123
  126.4 38.6 %all-gather.12.cloned.1.call-done = bf16[1,2048,1024]{2,1,0:T(8,128)(2,1)} async-done(((bf16[1,2048,128]{2,1,0:T(8,128)(2,1)}), bf16[1,2048,1024]{2,1,0:T(8,128)(2,1)}) %all-gather.12.cloned.1.call-update) | async-done | bytes 4194320 | tf_op jit(solution)/shard_map/all_gather | solution.py:121
  165.0 47.5 %all-gather.14.cloned.1.call-done = bf16[1,2048,1024]{2,1,0:T(8,128)(2,1)} async-done(((bf16[1,2048,128]{2,1,0:T(8,128)(2,1)}), bf16[1,2048,1024]{2,1,0:T(8,128)(2,1)}) %all-gather.14.cloned.1.call-update) | async-done | bytes 4194320 | tf_op jit(solution)/shard_map/all_gather | solution.py:122
  212.5 8.6 %fusion.26 = bf16[384,2048]{1,0:T(8,128)(2,1)} fusion(bf16[1,2048,1024]{2,1,0:T(8,128)(2,1)} %all-gather.14.cloned.1.call-done, f32[384,1024]{1,0:T(8,128)} %fusion.24, bf16[384,2048]{1,0:T(8,128)(2,1)S(1)} %bitcast.64, bf16[1,2048,1024]{2,1,0:T(8,128)(2,1)} %all-gather.12.cloned.1.call-done), kind=kOutput, calls=%fused_computation.41 | convolution fusion | flops 3224371200 | bytes 13107200 | tf_op jit(solution)/shard_map/jrf,jdf->jrd/dot_general | solution.py:128
  221.1 3.8 %all-to-all-start.1 = ((bf16[4,96,2048]{2,1,0:T(8,128)(2,1)}), bf16[4,96,2048]{2,1,0:T(8,128)(2,1)S(1)}, u32[]{:S(2)}, u32[]{:S(2)}) async-start(bf16[4,96,2048]{2,1,0:T(8,128)(2,1)} %bitcast.65), calls=%async_computation.2 | async-start | bytes 3145728 | tf_op jit(solution)/shard_map/all_to_all | solution.py:135
  224.9 0.1 copy.29
  225.0 19.7 %all-to-all-done.1 = bf16[4,96,2048]{2,1,0:T(8,128)(2,1)S(1)} async-done(((bf16[4,96,2048]{2,1,0:T(8,128)(2,1)}), bf16[4,96,2048]{2,1,0:T(8,128)(2,1)S(1)}, u32[]{:S(2)}, u32[]{:S(2)}) %all-to-all-start.1) | async-done | bytes 1572896 | tf_op jit(solution)/shard_map/all_to_all | solution.py:135
  244.7 2.3 gather_fusion.1
  247.1 2.4 reshape.163
  249.4 3.9 %multiply_reduce_fusion = bf16[128,2048]{1,0:T(8,128)(2,1)} fusion(f32[128,2,2048]{2,1,0:T(2,128)S(1)} %reshape.163, f32[128,2]{1,0:T(8,128)S(1)} %copy.29), kind=kLoop, calls=%fused_computation.42 | loop fusion | flops 786432 | bytes 2622464 | tf_op jit(solution)/shard_map/reduce_sum | solution.py:140
  (55 shorter events, 0.4 us)
Async XLA Ops:
  7.2 72.7 %copy-start = (bf16[2,128,2048]{2,1,0:T(8,128)(2,1)S(1)}, bf16[2,128,2048]{2,1,0:T(8,128)(2,1)}, u32[]{:S(2)}) copy-start(bf16[2,128,2048]{2,1,0:T(8,128)(2,1)} %param.23) | copy-start | bytes 3145732
  7.2 5.6 %copy-start.6 = (s32[128,2]{0,1:T(2,128)S(1)}, s32[128,2]{0,1:T(2,128)}, u32[]{:S(2)}) copy-start(s32[128,2]{0,1:T(2,128)} %param.26) | copy-start | bytes 3076
  7.2 6.0 %copy-start.4 = (bf16[512,2,128]{2,1,0:T(2,128)(2,1)S(1)}, bf16[512,2,128]{2,1,0:T(2,128)(2,1)}, u32[]{:S(2)}) copy-start(bf16[512,2,128]{2,1,0:T(2,128)(2,1)} %param.18) | copy-start | bytes 786436
  7.2 9.5 %copy-start.1 = (bf16[128,2048]{1,0:T(8,128)(2,1)S(1)}, bf16[128,2048]{1,0:T(8,128)(2,1)}, u32[]{:S(2)}) copy-start(bf16[128,2048]{1,0:T(8,128)(2,1)} %param.24) | copy-start | bytes 1572868
  7.2 32.5 %all-gather.6.cloned.1.call-start = ((), (), s32[]{:S(2)}) async-start(), calls=%async_computation.3 | async-start | bytes 1310720 | tf_op jit(solution)/shard_map/all_gather | solution.py:53
  9.1 7.9 %copy-start.5 = (f32[2048]{0:T(1024)S(1)}, f32[2048]{0:T(1024)}, u32[]{:S(2)}) copy-start(f32[2048]{0:T(1024)} %param.25) | copy-start | bytes 24580
  9.1 59.0 %all-gather.8.cloned.1.call-start = ((), (), s32[]{:S(2)}) async-start(), calls=%async_computation.4 | async-start | bytes 1310720 | tf_op jit(solution)/shard_map/all_gather | solution.py:54
  10.8 109.8 %all-gather.10.cloned.1.call-start = ((), (), s32[]{:S(2)}) async-start(), calls=%async_computation.6 | async-start | bytes 4718592 | tf_op jit(solution)/shard_map/all_gather | solution.py:120
  11.6 153.4 %all-gather.12.cloned.1.call-start = ((), (), s32[]{:S(2)}) async-start(), calls=%async_computation.7 | async-start | bytes 4718592 | tf_op jit(solution)/shard_map/all_gather | solution.py:121
  12.2 200.3 %all-gather.14.cloned.1.call-start = ((), (), s32[]{:S(2)}) async-start(), calls=%async_computation.8 | async-start | bytes 4718592 | tf_op jit(solution)/shard_map/all_gather | solution.py:122
  12.7 240.6 %reduce-scatter.2.cloned.1.call-start = ((), (), s32[]{:S(2)}) async-start(), calls=%async_computation.5 | async-start | bytes 2359296 | tf_op jit(solution)/shard_map/reduce_scatter | solution.py:81
  69.5 9.9 %copy-start.8 = (f32[2]{0:T(128)S(1)}, f32[2]{0:T(128)}, u32[]{:S(2)}) copy-start(f32[2]{0:T(128)} %param.21) | copy-start | bytes 28
  69.5 10.4 %copy-start.9 = (f32[128]{0:T(128)S(1)}, f32[128]{0:T(128)}, u32[]{:S(2)}) copy-start(f32[128]{0:T(128)} %param.22) | copy-start | bytes 1540
  79.9 2.2 copy-start.2
  120.7 91.8 %copy-start.3 = (bf16[4,96,2048]{2,1,0:T(8,128)(2,1)S(1)}, bf16[4,96,2048]{2,1,0:T(8,128)(2,1)}, u32[]{:S(2)}) copy-start(bf16[4,96,2048]{2,1,0:T(8,128)(2,1)} %all_to_all.10) | copy-start | bytes 4718596
  221.1 3.8 %copy-start.7 = (f32[128,2]{0,1:T(2,128)S(1)}, f32[128,2]{0,1:T(2,128)}, u32[]{:S(2)}) copy-start(f32[128,2]{0,1:T(2,128)} %param.28) | copy-start | bytes 3076
  221.1 3.8 %copy-start.10 = (f32[128]{0:T(128)S(1)}, f32[128]{0:T(128)}, u32[]{:S(2)}) copy-start(f32[128]{0:T(128)} %param.27) | copy-start | bytes 1540
  221.1 23.6 %all-to-all-start.1 = ((bf16[4,96,2048]{2,1,0:T(8,128)(2,1)}), bf16[4,96,2048]{2,1,0:T(8,128)(2,1)S(1)}, u32[]{:S(2)}, u32[]{:S(2)}) async-start(bf16[4,96,2048]{2,1,0:T(8,128)(2,1)} %bitcast.65), calls=%async_computation.2 | async-start | bytes 3145728 | tf_op jit(solution)/shard_map/all_to_all | solution.py:135
Sparse Core Ops, SparseCore 0:
  10.4 29.2 all-gather.5
  41.5 26.4 all-gather.7
  69.7 47.8 all-gather.9
  119.0 45.9 all-gather.11
  166.4 45.9 all-gather.13
  215.2 34.1 reduce-scatter.1
where the time goes:
time: 261 us; the launch traced here: 260 us
  waiting for transfers between devices  155 us (59%)
  blocking collectives  36.1 us (14%)
  local copies, waits for them, and re-layouts  20.4 us (8%)
  matrix products  19.2 us (7%)
  between operations  14.4 us (6%)
  other arithmetic  7.89 us (3%)
  starting transfers between devices  4.02 us (2%)
  loops' own time  2.93 us (1%)
    all_gather x1, waiting for transfers between devices, expert_half(): piece_down = lax.all_gather(down_weight, 'tp', axis=2, tiled=True)  47.5 us
    all_gather x1, waiting for transfers between devices, expert_half(): piece_up = lax.all_gather(up_weight, 'tp', axis=2, tiled=True)  38.6 us
    all_to_all x1, blocking collectives, expert_half(): lax.all_to_all(outgoing, 'ep', split_axis=0, concat_axis=0, tiled=True)  36.1 us
    all_gather x1, waiting for transfers between devices, attend_heads(): value_piece = lax.all_gather(values, 'ep', axis=0, tiled=True)  26.1 us
    all_gather x1, waiting for transfers between devices, attend_heads(): key_piece = lax.all_gather(keys, 'ep', axis=0, tiled=True)  21.8 us
    all_to_all x1, waiting for transfers between devices, expert_half(): lax.all_to_all(outbound, 'ep', split_axis=0, concat_axis=0, tiled=True)  19.7 us
    dot_general x1, matrix products, expert_half(): jnp.einsum('jrf,jdf->jrd', hidden, piece_down, preferred_element_type=jnp...  8.63 us
    unnamed x28, local copies, waits for them, and re-layouts  7.42 us
  transfers between devices with their start and end apart: 7, of which 5 were waited for; matrix products, arithmetic and copies ran while one was open for 18% of the time, Pallas kernels for 0%

commit v1 on v0

--- a/solution.py
+++ b/solution.py
@@ -5,6 +5,26 @@
 from jax.sharding import PartitionSpec as P
 
 HEAD = 64
+
+
+def kinds_show(piece_in, axis_id, x_local):
+    plain = lax.axis_index(axis_id)
+    current_arr = lax.axis_size(axis_id)
+    entries = []
+    arr_out, p_next, reached = (current_arr, plain, piece_in.shape[2])
+    b = 0
+    while b < arr_out:
+        entries.append((b, (b + 1) % arr_out))
+        b += 1
+    current_block, r2 = (piece_in, None)
+    dd = 0
+    while dd < arr_out:
+        front = lax.ppermute(current_block, axis_id, entries) if dd < arr_out - 1 else None
+        right_arr = x_local(current_block, (p_next - dd) % arr_out * reached)
+        r2 = right_arr if r2 is None else r2 + right_arr
+        current_block = front
+        dd += 1
+    return r2
 
 
 def attend_heads(queries, keys, values, mixing, head_gain):
@@ -119,14 +139,20 @@
     expert_rows = expert_rows.reshape(local_count, ep_count * capacity, width)
     piece_gate = lax.all_gather(gate_weight, "tp", axis=2, tiled=True)
     piece_up = lax.all_gather(up_weight, "tp", axis=2, tiled=True)
-    piece_down = lax.all_gather(down_weight, "tp", axis=2, tiled=True)
     gate_part = jnp.einsum(
         "jrd,jdf->jrf", expert_rows, piece_gate, preferred_element_type=jnp.float32
     )
     up_part = jnp.einsum("jrd,jdf->jrf", expert_rows, piece_up, preferred_element_type=jnp.float32)
     hidden = (jax.nn.silu(gate_part) * up_part).astype(jnp.bfloat16)
-    expert_out = jnp.einsum(
-        "jrf,jdf->jrd", hidden, piece_down, preferred_element_type=jnp.float32
+    expert_out = kinds_show(
+        down_weight,
+        "tp",
+        lambda part, offset_2: jnp.einsum(
+            "jrf,jdf->jrd",
+            lax.dynamic_slice_in_dim(hidden, offset_2, part.shape[2], axis=2),
+            part,
+            preferred_element_type=jnp.float32,
+        ),
     ).astype(jnp.bfloat16)
     outbound = jnp.transpose(
         expert_out.reshape(local_count, ep_count, capacity, width), (1, 0, 2, 3)

time: 261 us -> 238 us (0.912)
  blocking collectives: 36.1 us -> 0 us
  starting transfers between devices: 4.02 us -> 9.24 us
  matrix products: 19.2 us -> 24.3 us
  waiting for transfers between devices: 155 us -> 158 us
    ppermute x0 -> x7, waiting for transfers between devices: none -> 50 us  [kinds_show(): lax.ppermute(current_block, axis_id, entries)]
    all_gather x1 -> x0, waiting for transfers between devices: 47.5 us -> none  [expert_half(): piece_down = lax.all_gather(down_weight, 'tp', axis=2, tiled=True)]
    all_to_all x1 -> x0, blocking collectives: 36.1 us -> none  [expert_half(): lax.all_to_all(outgoing, 'ep', split_axis=0, concat_axis=0, tiled=True)]
    all_gather x1, waiting for transfers between devices: 0.01 us -> 26.8 us  [expert_half(): piece_gate = lax.all_gather(gate_weight, 'tp', axis=2, tiled=True)]
    all_gather x1, waiting for transfers between devices: 21.8 us -> 0.02 us  [attend_heads(): key_piece = lax.all_gather(keys, 'ep', axis=0, tiled=True)]
    all_gather x1, waiting for transfers between devices: 26.1 us -> 19.9 us  [attend_heads(): value_piece = lax.all_gather(values, 'ep', axis=0, tiled=True)]
    dot_general x1 -> x9, matrix products: 8.63 us -> 13.8 us  [the longest x8 8.7 us: expert_half(): jnp.einsum('jrf,jdf->jrd', lax.dynamic_slice_in_dim(hidden, offset_2, par...]
    all_to_all x0 -> x1, starting transfers between devices: none -> 4.51 us  [expert_half(): lax.all_to_all(outgoing, 'ep', split_axis=0, concat_axis=0, tiled=True)]
  transfers between devices with their start and end apart: 7 -> 14, of which waited for: 5 -> 9; matrix products, arithmetic and copies ran while one was open for 18% -> 21% of each run, Pallas kernels for 0% -> 0%
where the time goes in v1:
time: 238 us
  waiting for transfers between devices  158 us (66%)
  matrix products  24.3 us (10%)
  local copies, waits for them, and re-layouts  21.9 us (9%)
  between operations  14.3 us (6%)
  starting transfers between devices  9.24 us (4%)
  other arithmetic  7.1 us (3%)
  loops' own time  2.92 us (1%)
    ppermute x7, waiting for transfers between devices, kinds_show(): lax.ppermute(current_block, axis_id, entries)  50 us
    all_gather x1, waiting for transfers between devices, expert_half(): piece_up = lax.all_gather(up_weight, 'tp', axis=2, tiled=True)  40.3 us
    all_gather x1, waiting for transfers between devices, expert_half(): piece_gate = lax.all_gather(gate_weight, 'tp', axis=2, tiled=True)  26.8 us
    all_gather x1, waiting for transfers between devices, attend_heads(): value_piece = lax.all_gather(values, 'ep', axis=0, tiled=True)  19.9 us
    all_to_all x1, waiting for transfers between devices, expert_half(): lax.all_to_all(outbound, 'ep', split_axis=0, concat_axis=0, tiled=True)  19.6 us
    dot_general x8, matrix products, expert_half(): jnp.einsum('jrf,jdf->jrd', lax.dynamic_slice_in_dim(hidden, offset_2, par...  8.7 us
    unnamed x40, local copies, waits for them, and re-layouts  8.33 us
    dot_general x1, matrix products, expert_half(): jnp.einsum('jrd,jdf->jrf', expert_rows, piece_gate, preferred_element_typ...  5.69 us
  transfers between devices with their start and end apart: 14, of which 9 were waited for; matrix products, arithmetic and copies ran while one was open for 21% of the time, Pallas kernels for 0%

profile of v1, /device:TPU:0, one launch (start us, length us, event | category | flops | bytes accessed | tf_op | source)
XLA Modules:
  0.0 237.6 jit_solution(1039132844441037306)
XLA Ops:
  7.3 1.8 copy.24
  9.2 1.7 copy.25
  10.9 0.7 all-gather.9.cloned.1.call-update
  11.7 0.5 all-gather.11.cloned.1.call-update
  12.2 0.5 collective-permute-start
  12.7 0.1 copy.31
  12.9 0.1 eq.38
  13.0 0.2 fusion.26
  13.2 10.4 %collective-permute-done = bf16[1,2048,128]{2,1,0:T(8,128)(2,1)S(1)} collective-permute-done((bf16[1,2048,128]{2,1,0:T(8,128)(2,1)S(1)}, bf16[1,2048,128]{2,1,0:T(8,128)(2,1)S(1)}, u32[]{:S(2)}, u32[]{:S(2)}) %collective-permute-start) | collective-permute-done | bytes 524320 | tf_op jit(solution)/shard_map/ppermute | solution.py:22
  23.6 0.1 eq.34
  23.8 1.2 reduce-window.6
  25.0 0.1 slice.34
  25.1 0.1 copy.33
  25.2 0.1 copy.34
  25.3 0.1 copy.30
  25.4 0.1 mul.193
  25.6 0.2 fusion.28
  25.8 8.2 %collective-permute-done.1 = bf16[1,2048,128]{2,1,0:T(8,128)(2,1)S(1)} collective-permute-done((bf16[1,2048,128]{2,1,0:T(8,128)(2,1)S(1)}, bf16[1,2048,128]{2,1,0:T(8,128)(2,1)S(1)}, u32[]{:S(2)}, u32[]{:S(2)}) %collective-permute-start.1) | collective-permute-done | bytes 524320 | tf_op jit(solution)/shard_map/ppermute | solution.py:22
  34.1 10.3 %collective-permute-done.2 = bf16[1,2048,128]{2,1,0:T(8,128)(2,1)S(1)} collective-permute-done((bf16[1,2048,128]{2,1,0:T(8,128)(2,1)S(1)}, bf16[1,2048,128]{2,1,0:T(8,128)(2,1)S(1)}, u32[]{:S(2)}, u32[]{:S(2)}) %collective-permute-start.2) | collective-permute-done | bytes 524320 | tf_op jit(solution)/shard_map/ppermute | solution.py:22
  44.5 1.4 scatter_custom_fusion
  45.9 3.1 %gather_fusion = bf16[384,2048]{1,0:T(8,128)(2,1)} fusion(bf16[129,2048]{1,0:T(8,128)(2,1)S(1)} %concatenate.3, s32[1024]{0:T(1024)S(1)} %pad_clamp_fusion.1), kind=kCustom, calls=%fused_computation | custom fusion | bytes 3147264 | tf_op jit(solution)/shard_map/gather | solution.py:134
  49.0 4.5 %all-to-all-start = ((bf16[4,96,2048]{2,1,0:T(8,128)(2,1)}), bf16[4,96,2048]{2,1,0:T(8,128)(2,1)}, u32[]{:S(2)}, u32[]{:S(2)}) async-start(bf16[4,96,2048]{2,1,0:T(8,128)(2,1)} %bitcast.11), calls=%async_computation.1 | async-start | bytes 3145728 | tf_op jit(solution)/shard_map/all_to_all | solution.py:135
  53.6 1.4 collective-permute-done.3
  55.0 0.2 copy.27
  55.2 2.3 copy.26
  57.5 19.9 %all-gather.7.cloned.1.call-done = bf16[2048,2,128]{2,0,1:T(8,128)(2,1)} async-done(((bf16[512,2,128]{2,0,1:T(8,128)(2,1)}), bf16[2048,2,128]{2,0,1:T(8,128)(2,1)}) %all-gather.7.cloned.1.call-update) | async-done | bytes 1048592 | tf_op jit(solution)/shard_map/all_gather | solution.py:74
  77.4 1.3 copy.28
  78.8 9.8 %while.23 = (s32[]{:T(128)}, f32[2,512]{1,0:T(2,128)S(1)}, f32[2,512]{1,0:T(2,128)S(1)}, f32[2,512,128]{2,1,0:T(8,128)S(1)}, f32[2,512]{1,0:T(2,128)S(1)}, /*ind...) while((s32[]{:T(128)}, f32[2,512]{1,0:T(2,128)S(1)}, ...), condition=%wide.region_7.8_spmd.clone, body=%wide.region_0.7_spmd.clone.sunk | while | flops 410784768 | bytes 17183128 | solution.py:90
  78.9 0.6 dynamic_slice.44
  80.1 4.6 %conditional.3 = ((f32[2,512]{1,0:T(2,128)S(1)}, f32[2,512]{1,0:T(2,128)S(1)}, f32[2,512,128]{2,1,0:T(8,128)S(1)}, f32[2,512]{1,0:T(2,128)S(1)}, f32[2,512]{1,0:T(2,128)S(1)}, /*index=5*/f32[2,512,128]{2,1,0:T(8,128)S(1)})) conditional(s32[]{:T(128)} %convert_element_type.85, (f32[2,512]{1,0:T(2,128)S(1)}, f32[2,512]{1,0:T(2,128)S(1)}, ...), branch_computations={%region_1.1_spmd, %region_2.6_spmd} | conditional | flops 410784768 | bytes 17180748 | solution.py:82
  80.1 1.0 dynamic-slice_bitcast_fusion
  81.1 0.2 broadcast_compare_fusion
  81.3 0.6 fusion.67
  82.0 0.3 fusion.3
  82.3 0.6 fusion.68
  82.9 0.3 fusion.5
  83.3 0.7 convolution_add_fusion
  84.0 0.7 convolution_add_fusion.1
  84.8 0.6 dynamic_slice.44
  86.1 0.6 dynamic_slice.44
  87.4 0.6 dynamic_slice.44
  88.7 0.5 multiply_reduce_fusion.1
  89.3 2.1 bitcast_convert_fusion
  91.5 19.8 %collective-permute-done.5 = bf16[1,2048,128]{2,1,0:T(8,128)(2,1)S(1)} collective-permute-done((bf16[1,2048,128]{2,1,0:T(8,128)(2,1)}, bf16[1,2048,128]{2,1,0:T(8,128)(2,1)S(1)}, u32[]{:S(2)}, u32[]{:S(2)}) %collective-permute-start.5) | collective-permute-done | bytes 524320 | tf_op jit(solution)/shard_map/ppermute | solution.py:22
  111.2 26.8 %all-gather.9.cloned.1.call-done = bf16[1,2048,1024]{2,1,0:T(8,128)(2,1)} async-done(((bf16[1,2048,128]{2,1,0:T(8,128)(2,1)}), bf16[1,2048,1024]{2,1,0:T(8,128)(2,1)}) %all-gather.9.cloned.1.call-update) | async-done | bytes 4194320 | tf_op jit(solution)/shard_map/all_gather | solution.py:140
  138.0 5.7 %fusion.22 = f32[384,1024]{1,0:T(8,128)} fusion(bf16[384,2048]{1,0:T(8,128)(2,1)} %bitcast.12, bf16[1,2048,1024]{2,1,0:T(8,128)(2,1)} %all-gather.9.cloned.1.call-done), kind=kOutput, calls=%fused_computation.36 | convolution fusion | flops 1610612736 | bytes 7340032 | tf_op jit(solution)/shard_map/jrd,jdf->jrf/dot_general | solution.py:142
  143.7 40.3 %all-gather.11.cloned.1.call-done = bf16[1,2048,1024]{2,1,0:T(8,128)(2,1)} async-done(((bf16[1,2048,128]{2,1,0:T(8,128)(2,1)}), bf16[1,2048,1024]{2,1,0:T(8,128)(2,1)}) %all-gather.11.cloned.1.call-update) | async-done | bytes 4194320 | tf_op jit(solution)/shard_map/all_gather | solution.py:141
  184.0 5.0 %multiply_convert_fusion = bf16[384,1024]{1,0:T(8,128)(2,1)S(1)} fusion(f32[384,1024]{1,0:T(8,128)} %fusion.22, bf16[384,2048]{1,0:T(8,128)(2,1)} %bitcast.12, bf16[1,2048,1024]{2,1,0:T(8,128)(2,1)} %all-gather.11.cloned.1.call-done), kind=kOutput, calls=%fused_computation.41 | convolution fusion | flops 1612972032 | bytes 8126464 | tf_op jit(solution)/shard_map/jrd,jdf->jrf/dot_general | solution.py:145
  189.1 0.6 fusion.42
  189.7 0.6 fusion.30
  190.3 1.7 fusion.32
  191.9 1.7 fusion.34
  193.6 0.6 fusion.36
  194.2 0.5 copy-done.7
  194.7 0.6 fusion.38
  195.3 0.5 copy-done.5
  195.7 0.6 fusion.40
  196.3 2.5 %add_convert_fusion = bf16[384,2048]{1,0:T(8,128)(2,1)} fusion(f32[384,2048]{1,0:T(8,128)S(1)} %fusion.30, f32[384,2048]{1,0:T(8,128)S(1)} %fusion.32, f32[384,2048]{1,0:T(8,128)S(1)} %fusion.34, f32[384,2048]{1,0:T(8,128)S(1)} %fusion.36, f32[384,2048]{1,0:T(8,128)S(1)} %fusion.38, f32[384,2048]{1,0:T(8,128)S(1)} %fusion.42, f32[384,2048]{1,0:T(8,128)S(1)} %fusion.40, ...), kind=kOutput, calls=%fused_computation.39 | convolution fusion | flops 207618048 | bytes 24215556 | tf_op jit(solution)/shard_map/jrf,jdf->jrd/dot_general | solution.py:150
  198.8 3.9 %all-to-all-start.1 = ((bf16[4,96,2048]{2,1,0:T(8,128)(2,1)}), bf16[4,96,2048]{2,1,0:T(8,128)(2,1)S(1)}, u32[]{:S(2)}, u32[]{:S(2)}) async-start(bf16[4,96,2048]{2,1,0:T(8,128)(2,1)} %bitcast.79), calls=%async_computation.2 | async-start | bytes 3145728 | tf_op jit(solution)/shard_map/all_to_all | solution.py:161
  202.8 0.1 copy.29
  202.9 19.6 %all-to-all-done.1 = bf16[4,96,2048]{2,1,0:T(8,128)(2,1)S(1)} async-done(((bf16[4,96,2048]{2,1,0:T(8,128)(2,1)}), bf16[4,96,2048]{2,1,0:T(8,128)(2,1)S(1)}, u32[]{:S(2)}, u32[]{:S(2)}) %all-to-all-start.1) | async-done | bytes 1572896 | tf_op jit(solution)/shard_map/all_to_all | solution.py:161
  222.5 2.3 gather_fusion.1
  224.8 2.4 reshape.227
  227.2 3.9 %multiply_reduce_fusion = bf16[128,2048]{1,0:T(8,128)(2,1)} fusion(f32[128,2,2048]{2,1,0:T(2,128)S(1)} %reshape.227, f32[128,2]{1,0:T(8,128)S(1)} %copy.29), kind=kLoop, calls=%fused_computation.40 | loop fusion | flops 786432 | bytes 2622464 | tf_op jit(solution)/shard_map/reduce_sum | solution.py:166
  (87 shorter events, 0.9 us)
Async XLA Ops:
  7.2 82.1 %copy-start = (bf16[2,128,2048]{2,1,0:T(8,128)(2,1)S(1)}, bf16[2,128,2048]{2,1,0:T(8,128)(2,1)}, u32[]{:S(2)}) copy-start(bf16[2,128,2048]{2,1,0:T(8,128)(2,1)} %param.23) | copy-start | bytes 3145732
  7.2 5.0 %copy-start.2 = (bf16[1,2048,128]{2,1,0:T(8,128)(2,1)S(1)}, bf16[1,2048,128]{2,1,0:T(8,128)(2,1)}, u32[]{:S(2)}) copy-start(bf16[1,2048,128]{2,1,0:T(8,128)(2,1)} %param.31) | copy-start | bytes 1572868
  7.2 5.5 %copy-start.12 = (s32[128,2]{0,1:T(2,128)S(1)}, s32[128,2]{0,1:T(2,128)}, u32[]{:S(2)}) copy-start(s32[128,2]{0,1:T(2,128)} %param.26) | copy-start | bytes 3076
  7.2 5.8 %copy-start.1 = (bf16[128,2048]{1,0:T(8,128)(2,1)S(1)}, bf16[128,2048]{1,0:T(8,128)(2,1)}, u32[]{:S(2)}) copy-start(bf16[128,2048]{1,0:T(8,128)(2,1)} %param.24) | copy-start | bytes 1572868
  7.2 18.4 %copy-start.11 = (f32[2048]{0:T(1024)S(1)}, f32[2048]{0:T(1024)}, u32[]{:S(2)}) copy-start(f32[2048]{0:T(1024)} %param.25) | copy-start | bytes 24580
  7.2 48.0 %all-gather.5.cloned.1.call-start = ((), (), s32[]{:S(2)}) async-start(), calls=%async_computation.3 | async-start | bytes 1310720 | tf_op jit(solution)/shard_map/all_gather | solution.py:73
  9.1 68.3 %all-gather.7.cloned.1.call-start = ((), (), s32[]{:S(2)}) async-start(), calls=%async_computation.4 | async-start | bytes 1310720 | tf_op jit(solution)/shard_map/all_gather | solution.py:74
  10.9 127.2 %all-gather.9.cloned.1.call-start = ((), (), s32[]{:S(2)}) async-start(), calls=%async_computation.6 | async-start | bytes 4718592 | tf_op jit(solution)/shard_map/all_gather | solution.py:140
  11.6 172.4 %all-gather.11.cloned.1.call-start = ((), (), s32[]{:S(2)}) async-start(), calls=%async_computation.7 | async-start | bytes 4718592 | tf_op jit(solution)/shard_map/all_gather | solution.py:141
  12.2 11.4 %collective-permute-start = (bf16[1,2048,128]{2,1,0:T(8,128)(2,1)S(1)}, bf16[1,2048,128]{2,1,0:T(8,128)(2,1)S(1)}, u32[]{:S(2)}, u32[]{:S(2)}) collective-permute-start(bf16[1,2048,128]{2,1,0:T(8,128)(2,1)S(1)} %copy-done.2), channel_id=1, source_target_pairs={{0,1},{1,2},{2,3},{3,4},{4,5},{5,6},{6,7},{7,0},{8,9},{9,10},{10,1... | collective-permute-start | bytes 1572872 | tf_op jit(solution)/shard_map/ppermute | solution.py:22
  23.6 25.4 %copy-start.4 = (bf16[1,2048,128]{2,1,0:T(8,128)(2,1)}, bf16[1,2048,128]{2,1,0:T(8,128)(2,1)S(1)}, u32[]{:S(2)}) copy-start(bf16[1,2048,128]{2,1,0:T(8,128)(2,1)S(1)} %collective-permute-done) | copy-start | bytes 1572868
  23.6 10.4 %collective-permute-start.1 = (bf16[1,2048,128]{2,1,0:T(8,128)(2,1)S(1)}, bf16[1,2048,128]{2,1,0:T(8,128)(2,1)S(1)}, u32[]{:S(2)}, u32[]{:S(2)}) collective-permute-start(bf16[1,2048,128]{2,1,0:T(8,128)(2,1)S(1)} %collective-permute-done), channel_id=1, source_target_pairs={{0,1},{1,2},{2,3},{3,4},{4,5},{5,6},{6,7},{7,0},{8,9},{9,10},{10,1... | collective-permute-start | bytes 1572872 | tf_op jit(solution)/shard_map/ppermute | solution.py:22
  34.0 15.0 %copy-start.6 = (bf16[1,2048,128]{2,1,0:T(8,128)(2,1)}, bf16[1,2048,128]{2,1,0:T(8,128)(2,1)S(1)}, u32[]{:S(2)}) copy-start(bf16[1,2048,128]{2,1,0:T(8,128)(2,1)S(1)} %collective-permute-done.1) | copy-start | bytes 1572868
  34.0 10.4 %collective-permute-start.2 = (bf16[1,2048,128]{2,1,0:T(8,128)(2,1)S(1)}, bf16[1,2048,128]{2,1,0:T(8,128)(2,1)S(1)}, u32[]{:S(2)}, u32[]{:S(2)}) collective-permute-start(bf16[1,2048,128]{2,1,0:T(8,128)(2,1)S(1)} %collective-permute-done.1), channel_id=1, source_target_pairs={{0,1},{1,2},{2,3},{3,4},{4,5},{5,6},{6,7},{7,0},{8,9},{9,10},{10,1... | collective-permute-start | bytes 1572872 | tf_op jit(solution)/shard_map/ppermute | solution.py:22
  44.4 4.6 %copy-start.8 = (bf16[1,2048,128]{2,1,0:T(8,128)(2,1)}, bf16[1,2048,128]{2,1,0:T(8,128)(2,1)S(1)}, u32[]{:S(2)}) copy-start(bf16[1,2048,128]{2,1,0:T(8,128)(2,1)S(1)} %collective-permute-done.2) | copy-start | bytes 1572868
  44.4 10.5 %collective-permute-start.3 = (bf16[1,2048,128]{2,1,0:T(8,128)(2,1)S(1)}, bf16[1,2048,128]{2,1,0:T(8,128)(2,1)}, u32[]{:S(2)}, u32[]{:S(2)}) collective-permute-start(bf16[1,2048,128]{2,1,0:T(8,128)(2,1)S(1)} %collective-permute-done.2), channel_id=1, source_target_pairs={{0,1},{1,2},{2,3},{3,4},{4,5},{5,6},{6,7},{7,0},{8,9},{9,10},{10,1... | collective-permute-start | bytes 1572872 | tf_op jit(solution)/shard_map/ppermute | solution.py:22
  49.0 5.9 %copy-start.10 = (bf16[512,2,128]{2,1,0:T(2,128)(2,1)S(1)}, bf16[512,2,128]{2,1,0:T(2,128)(2,1)}, u32[]{:S(2)}) copy-start(bf16[512,2,128]{2,1,0:T(2,128)(2,1)} %param.18) | copy-start | bytes 786436
  49.0 62.2 %all-to-all-start = ((bf16[4,96,2048]{2,1,0:T(8,128)(2,1)}), bf16[4,96,2048]{2,1,0:T(8,128)(2,1)}, u32[]{:S(2)}, u32[]{:S(2)}) async-start(bf16[4,96,2048]{2,1,0:T(8,128)(2,1)} %bitcast.11), calls=%async_computation.1 | async-start | bytes 3145728 | tf_op jit(solution)/shard_map/all_to_all | solution.py:135
  53.6 177.5 %reduce-scatter.2.cloned.1.call-start = ((), (), s32[]{:S(2)}) async-start(), calls=%async_computation.5 | async-start | bytes 2359296 | tf_op jit(solution)/shard_map/reduce_scatter | solution.py:101
  55.0 34.2 %collective-permute-start.4 = (bf16[1,2048,128]{2,1,0:T(8,128)(2,1)}, bf16[1,2048,128]{2,1,0:T(8,128)(2,1)}, u32[]{:S(2)}, u32[]{:S(2)}) collective-permute-start(bf16[1,2048,128]{2,1,0:T(8,128)(2,1)} %collective-permute-done.3), channel_id=1, source_target_pairs={{0,1},{1,2},{2,3},{3,4},{4,5},{5,6},{6,7},{7,0},{8,9},{9,10},{10,1... | collective-permute-start | bytes 1572872 | tf_op jit(solution)/shard_map/ppermute | solution.py:22
  78.8 9.9 %copy-start.14 = (f32[2]{0:T(128)S(1)}, f32[2]{0:T(128)}, u32[]{:S(2)}) copy-start(f32[2]{0:T(128)} %param.21) | copy-start | bytes 28
  78.8 10.5 %copy-start.15 = (f32[128]{0:T(128)S(1)}, f32[128]{0:T(128)}, u32[]{:S(2)}) copy-start(f32[128]{0:T(128)} %param.22) | copy-start | bytes 1540
  89.2 22.0 %collective-permute-start.5 = (bf16[1,2048,128]{2,1,0:T(8,128)(2,1)}, bf16[1,2048,128]{2,1,0:T(8,128)(2,1)S(1)}, u32[]{:S(2)}, u32[]{:S(2)}) collective-permute-start(bf16[1,2048,128]{2,1,0:T(8,128)(2,1)} %collective-permute-done.4), channel_id=1, source_target_pairs={{0,1},{1,2},{2,3},{3,4},{4,5},{5,6},{6,7},{7,0},{8,9},{9,10},{10,1... | collective-permute-start | bytes 1572872 | tf_op jit(solution)/shard_map/ppermute | solution.py:22
  111.2 85.1 %collective-permute-start.6 = (bf16[1,2048,128]{2,1,0:T(8,128)(2,1)S(1)}, bf16[1,2048,128]{2,1,0:T(8,128)(2,1)S(1)}, u32[]{:S(2)}, u32[]{:S(2)}) collective-permute-start(bf16[1,2048,128]{2,1,0:T(8,128)(2,1)S(1)} %collective-permute-done.5), channel_id=1, source_target_pairs={{0,1},{1,2},{2,3},{3,4},{4,5},{5,6},{6,7},{7,0},{8,9},{9,10},{10,1... | collective-permute-start | bytes 1572872 | tf_op jit(solution)/shard_map/ppermute | solution.py:22
  143.7 45.4 %copy-start.3 = (bf16[1,2048,128]{2,1,0:T(8,128)(2,1)S(1)}, bf16[1,2048,128]{2,1,0:T(8,128)(2,1)}, u32[]{:S(2)}) copy-start(bf16[1,2048,128]{2,1,0:T(8,128)(2,1)} %param.31) | copy-start | bytes 1572868
  191.9 1.7 copy-start.9
  193.6 1.0 copy-start.7
  194.7 1.0 copy-start.5
  198.8 3.9 %copy-start.13 = (f32[128,2]{0,1:T(2,128)S(1)}, f32[128,2]{0,1:T(2,128)}, u32[]{:S(2)}) copy-start(f32[128,2]{0,1:T(2,128)} %param.28) | copy-start | bytes 3076
  198.8 3.9 %copy-start.16 = (f32[128]{0:T(128)S(1)}, f32[128]{0:T(128)}, u32[]{:S(2)}) copy-start(f32[128]{0:T(128)} %param.27) | copy-start | bytes 1540
  198.8 23.7 %all-to-all-start.1 = ((bf16[4,96,2048]{2,1,0:T(8,128)(2,1)}), bf16[4,96,2048]{2,1,0:T(8,128)(2,1)S(1)}, u32[]{:S(2)}, u32[]{:S(2)}) async-start(bf16[4,96,2048]{2,1,0:T(8,128)(2,1)} %bitcast.79), calls=%async_computation.2 | async-start | bytes 3145728 | tf_op jit(solution)/shard_map/all_to_all | solution.py:161
Sparse Core Ops, SparseCore 0:
  10.5 29.2 all-gather.4
  41.6 35.7 all-gather.6
  79.0 59.0 all-gather.8
  139.5 44.5 all-gather.10
  186.7 34.1 reduce-scatter.1
